TPU v7x, 512 devices: a whole 4x4x16 slice. The times are simulated.
512 devices in a mesh: dp: 4 (over x), kv: 64 (over z, y), tp: 2 (over core).
Axes of the slice: x: 4, y: 4, z: 16, core: 2. Of those that a mesh axis runs over, the one named last changes fastest.
Arguments:
- tokens: bfloat16 [65536, 4096], P(('dp', 'kv')), parts along dimension 0, may hold values from -16 to 16
- query_weight: bfloat16 [4096, 1024], P('kv', 'tp'), may hold values from -0.09375 to 0.09375
- key_weight: bfloat16 [4096, 256], P('kv', 'tp'), may hold values from -0.09375 to 0.09375
- value_weight: bfloat16 [4096, 256], P('kv', 'tp'), may hold values from -0.09375 to 0.09375
- out_weight: bfloat16 [1024, 4096], P('kv', 'tp'), may hold values from -1.5 to 1.5
- chosen: int32 [2048, 16], P(('dp', 'kv')), parts along dimension 0, may hold values from -1 to 511, as said below
- live_length: int32 [4], P('dp'), parts along dimension 0, may hold values from 2048 to 16384
Outputs:
- mixed: bfloat16 [65536, 4096], P(('dp', 'kv'), 'tp'), parts along dimension 0
There are 4 independent parts, one for each index of `dp`. A program takes and returns all parts, laid end to end along the dimension named above; an argument that names none is the same for every part. Nothing has to cross between parts.
Inputs may be any that keep to these rules, and one draw needn't show every extreme that they name: `chosen`: row j lists 16 entries: entry 0 is j itself, the others are distinct blocks before j, or -1 for unused entries. The query blocks of one device together read at most 2 distinct blocks held by any one other device, and some device reads 2 of another's in every draw.
All inputs are finite; a program needn't handle non-finite values.
Results may differ from a plain program's by a relative error of at most 0.0085.
Values may be sent and summed in bfloat16 or wider, within the bound.
No kernel may reach another device: no remote copies, remote signals or barrier semaphores. Data moves between devices by JAX's collectives and lax.ppermute only.
A program may use at most 64 MiB of HBM per device.

v0:
```python
import jax
import jax.numpy as jnp
from jax import lax
from jax.sharding import Mesh
from jax.sharding import PartitionSpec as P

HD = 128
BLOCK = 32
CAP = 2
KV = ("kv_0", "kv_1")
DP_KV = ("dp", "kv_0", "kv_1")


def side_by_side(arrays, axis, dim, along):
    both = jnp.concatenate(arrays, axis=along)
    filled, at, outs = (lax.all_gather(both, axis, axis=dim, tiled=True), 0, [])
    for a in arrays:
        outs.append(lax.slice_in_dim(filled, at, at + a.shape[along], axis=along))
        at += a.shape[along]
    return tuple(outs)


def copy_for_each(shard, axis):
    count = lax.axis_size(axis)
    return lax.all_to_all(
        jnp.broadcast_to(shard[None], (count, *shard.shape)), axis, 0, 0, tiled=True
    )


def laid_out(blocks, dim):
    lengths = list(blocks.shape[1:])
    lengths[dim] *= blocks.shape[0]
    return jnp.moveaxis(blocks, 0, dim).reshape(lengths)


def gathered_copies(shard, axis, dim):
    blocks = copy_for_each(shard, axis)
    return laid_out(blocks, dim)


def gathered_by_axis(shard, axes, dim):
    for axis in reversed(axes):
        shard = lax.all_gather(shard, axis, axis=dim, tiled=True)
    return shard


def body(tokens, query_weight, key_weight, value_weight, out_weight, chosen, live_length):
    rows = tokens.shape[0]
    per_dev = rows // BLOCK
    owners = lax.axis_size(KV)
    me = lax.axis_index(KV)

    def add_rows(piece):
        return jnp.dot(tokens, piece, preferred_element_type=jnp.float32)

    pieces = side_by_side((query_weight, key_weight, value_weight), KV, 0, 1)
    queries = add_rows(pieces[0])
    keys = add_rows(pieces[1])
    values = add_rows(pieces[2])
    queries = queries.astype(jnp.bfloat16)
    paired = jnp.concatenate([keys.astype(jnp.bfloat16), values.astype(jnp.bfloat16)], axis=1)
    width = paired.shape[1]
    local_blocks = paired.reshape(per_dev, BLOCK, width)
    valid = chosen >= 0
    safe = jnp.maximum(chosen, 0)
    blocks_all = owners * per_dev
    hits = (safe[:, :, None] == jnp.arange(blocks_all, dtype=jnp.int32)[None, None, :]) & valid[
        :, :, None
    ]
    needed = jnp.any(hits, axis=(0, 1)).reshape(owners, per_dev)
    needed = needed & (jnp.arange(owners, dtype=jnp.int32) != me)[:, None]
    ranks = jnp.cumsum(needed.astype(jnp.int32), axis=1)
    local_ids = jnp.arange(per_dev, dtype=jnp.int32)
    slot_lists = []
    for slot in range(CAP):
        marked = needed & (ranks == slot + 1)
        found = jnp.any(marked, axis=1)
        where_at = jnp.sum(jnp.where(marked, local_ids[None, :], 0), axis=1)
        slot_lists.append(jnp.where(found, where_at, -1))
    wanted = jnp.stack(slot_lists, axis=1)
    requested = lax.all_to_all(wanted, KV, split_axis=0, concat_axis=0, tiled=True)
    outgoing = local_blocks[jnp.maximum(requested, 0)]
    outgoing = jnp.where((requested >= 0)[:, :, None, None], outgoing, jnp.zeros((), jnp.bfloat16))
    incoming = lax.all_to_all(outgoing, KV, split_axis=0, concat_axis=0, tiled=True)
    table = jnp.concatenate([incoming.reshape(owners * CAP, BLOCK, width), local_blocks], axis=0)
    segment_retainer = safe // per_dev
    local_of = safe % per_dev
    match = (wanted[None, None, :, :] == local_of[:, :, None, None]) & (
        jnp.arange(owners, dtype=jnp.int32)[None, None, :, None]
        == segment_retainer[:, :, None, None]
    )
    slot_index = jnp.arange(owners * CAP, dtype=jnp.int32).reshape(owners, CAP)
    remote_at = jnp.sum(jnp.where(match, slot_index[None, None], 0), axis=(2, 3))
    position = jnp.where(segment_retainer == me, owners * CAP + local_of, remote_at)
    picked = table[position]
    near_keys = picked[..., :HD]
    near_values = picked[..., HD:]
    grouped = queries.reshape(per_dev, BLOCK, -1, HD)
    scores = jnp.einsum(
        "jqhd,jnbd->jhqnb", grouped, near_keys, preferred_element_type=jnp.float32
    ) * HD ** (-0.5)
    query_pos = (me * per_dev + jnp.arange(per_dev, dtype=jnp.int32))[:, None] * BLOCK + jnp.arange(
        BLOCK, dtype=jnp.int32
    )[None, :]
    key_pos = safe[:, :, None] * BLOCK + jnp.arange(BLOCK, dtype=jnp.int32)[None, None, :]
    allowed = valid[:, None, :, None] & (key_pos[:, None, :, :] <= query_pos[:, :, None, None])
    masked = jnp.where(allowed[:, None], scores, -jnp.inf)
    top = jnp.max(masked, axis=(3, 4), keepdims=True)
    weights = jnp.exp(masked - top)
    total = jnp.sum(weights, axis=(3, 4))
    summed = jnp.einsum(
        "jhqnb,jnbd->jqhd",
        weights.astype(jnp.bfloat16),
        near_values,
        preferred_element_type=jnp.float32,
    )
    result = summed / jnp.transpose(total, (0, 2, 1))[..., None]
    live = query_pos < live_length[0]
    result = jnp.where(live[:, :, None, None], result, 0.0)
    attended = result.astype(jnp.bfloat16).reshape(rows, -1)
    every_head = gathered_copies(attended, "tp", 1)
    mixed = jnp.dot(
        every_head, gathered_by_axis(out_weight, KV, 0), preferred_element_type=jnp.float32
    )
    return mixed.astype(jnp.bfloat16)


def solution(mesh):
    split = Mesh(
        mesh.devices.reshape(mesh.shape["dp"], 16, 4, mesh.shape["tp"]),
        ("dp", "kv_0", "kv_1", "tp"),
    )
    placed = (
        P(DP_KV, None),
        P(KV, "tp"),
        P(KV, "tp"),
        P(KV, "tp"),
        P(KV, "tp"),
        P(DP_KV, None),
        P("dp"),
    )
    return jax.shard_map(
        body, mesh=split, in_specs=placed, out_specs=P(DP_KV, "tp"), check_vma=False
    )
```

profile of v0, /device:TPU:2, one launch (start us, length us, event | category | flops | bytes accessed | tf_op | source)
XLA Modules:
  0.0 335.5 jit_solution(2070661403445343551)
XLA Ops:
  7.4 1.7 pad_maximum_fusion.2
  9.1 0.7 broadcast_compare_fusion.1
  9.8 0.7 add_select_fusion.1
  10.5 0.1 fusion.33
  10.8 0.2 reduce_window_sum.11
  10.9 0.2 select_reduce_fusion.2
  11.5 33.3 %all_to_all.19 = s32[64,1,2]{2,1,0:T(1,128)S(1)} all-to-all(s32[64,1,2]{2,1,0:T(1,128)S(1)} %copy.32), channel_id=1, replica_groups=mesh['dp'=4,'kv_0'=16,'kv_1'=4,'tp'=2] {'kv_0','kv_1'}, dimensions={0} | all-to-all | bytes 1024 | tf_op jit(solution)/shard_map/all_to_all | solution.py:81
  44.9 0.1 reshape.151
  45.1 0.1 copy.34
  45.3 121.0 %all-gather.3.cloned.1.call-done = bf16[4096,768]{1,0:T(8,128)(2,1)} async-done(((bf16[64,768]{1,0:T(8,128)(2,1)}), bf16[4096,768]{1,0:T(8,128)(2,1)}) %all-gather.3.cloned.1.call-update) | async-done | bytes 6291472 | tf_op jit(solution)/shard_map/all_gather | solution.py:16
  166.3 2.1 fusion.17
  168.3 2.1 fusion.18
  170.5 2.0 gather_fusion
  172.6 3.2 broadcast_select_fusion
  175.7 10.1 %all-to-all-start.1 = ((bf16[64,2,32,256]{3,2,1,0:T(8,128)(2,1)}), bf16[64,2,32,256]{3,2,1,0:T(8,128)(2,1)}, u32[]{:S(2)}, u32[]{:S(2)}) async-start(bf16[64,2,32,256]{3,2,1,0:T(8,128)(2,1)} %broadcast_select_fusion), calls=%async_computation.1 | async-start | bytes 4194304 | tf_op jit(solution)/shard_map/all_to_all | solution.py:84
  185.9 14.0 %all_gather.10 = bf16[64,2048]{1,0:T(8,128)(2,1)} all-gather(bf16[16,2048]{1,0:T(8,128)(2,1)S(1)} %copy-done.2), channel_id=1, replica_groups=mesh['dp'=4,'kv_0'=16,'kv_1'=4,'tp'=2] {'kv_1'}, dimensions={0}, use_global_device_ids=true | all-gather | bytes 327680 | tf_op jit(solution)/shard_map/all_gather | solution.py:43
  200.0 0.3 select_reduce_fusion
  201.3 1.0 compare_and_fusion
  202.3 3.5 %fusion.14 = bf16[256,512]{0,1:T(8,128)(2,1)S(1)} fusion(bf16[256,4096]{1,0:T(8,128)(2,1)S(1)} %copy-done, bf16[4096,768]{1,0:T(8,128)(2,1)} %all-gather.3.cloned.1.call-done), kind=kOutput, calls=%fused_computation.17 | convolution fusion | flops 1073872896 | bytes 6553600 | tf_op jit(solution)/shard_map/dot_general | solution.py:54
  205.8 0.1 copy.36
  206.0 86.4 %all-to-all-done.1 = bf16[64,2,32,256]{3,2,1,0:T(8,128)(2,1)} async-done(((bf16[64,2,32,256]{3,2,1,0:T(8,128)(2,1)}), bf16[64,2,32,256]{3,2,1,0:T(8,128)(2,1)}, u32[]{:S(2)}, u32[]{:S(2)}) %all-to-all-start.1) | async-done | bytes 2097184 | tf_op jit(solution)/shard_map/all_to_all | solution.py:84
  292.5 3.2 pad_maximum_fusion
  295.7 3.6 %gather_fusion.1 = bf16[128,32,256]{2,1,0:T(8,128)(2,1)} fusion(bf16[136,32,256]{2,1,0:T(8,128)(2,1)} %pad_maximum_fusion, s32[1024]{0:T(1024)S(1)} %pad_clamp_fusion), kind=kCustom, calls=%fused_computation.1 | custom fusion | bytes 4194816 | tf_op jit(solution)/shard_map/gather | solution.py:95
  299.3 2.9 fusion.2
  302.2 2.5 fusion
  304.8 2.2 fusion.28
  306.9 0.1 copy.39
  307.1 0.1 copy.40
  307.3 0.8 broadcast_in_dim.118
  308.1 3.5 %all-to-all-start.2 = ((bf16[2,256,512]{1,2,0:T(8,128)(2,1)}), bf16[2,256,512]{1,2,0:T(8,128)(2,1)S(1)}, u32[]{:S(2)}, u32[]{:S(2)}) async-start(bf16[2,256,512]{1,2,0:T(8,128)(2,1)} %broadcast_in_dim.118), calls=%async_computation.2 | async-start | bytes 1048576 | tf_op jit(solution)/shard_map/all_to_all | solution.py:25
  311.6 12.0 %all-gather.5.cloned.1.call-done = bf16[1024,2048]{1,0:T(8,128)(2,1)} async-done(((bf16[64,2048]{1,0:T(8,128)(2,1)}), bf16[1024,2048]{1,0:T(8,128)(2,1)}) %all-gather.5.cloned.1.call-update) | async-done | bytes 4194320 | tf_op jit(solution)/shard_map/all_gather | solution.py:43
  323.6 4.4 %convolution_convert_fusion = bf16[256,2048]{1,0:T(8,128)(2,1)} fusion(bf16[256,1024]{0,1:T(8,128)(2,1)S(1)} %bitcast.91, bf16[1024,2048]{1,0:T(8,128)(2,1)} %all-gather.5.cloned.1.call-done), kind=kOutput, calls=%fused_computation.11 | convolution fusion | flops 1074266112 | bytes 5767168 | tf_op jit(solution)/shard_map/dot_general | solution.py:122
  (38 shorter events, 1.5 us)
Async XLA Ops:
  7.4 158.9 %copy-start = (bf16[256,4096]{1,0:T(8,128)(2,1)S(1)}, bf16[256,4096]{1,0:T(8,128)(2,1)}, u32[]{:S(2)}) copy-start(bf16[256,4096]{1,0:T(8,128)(2,1)} %param.7) | copy-start | bytes 6291460
  7.4 158.9 %all-gather.3.cloned.1.call-start = ((), (), s32[]{:S(2)}) async-start(), calls=%async_computation.3 | async-start | bytes 6389760 | tf_op jit(solution)/shard_map/all_gather | solution.py:16
  175.7 10.1 %copy-start.2 = (bf16[16,2048]{1,0:T(8,128)(2,1)S(1)}, bf16[16,2048]{1,0:T(8,128)(2,1)}, u32[]{:S(2)}) copy-start(bf16[16,2048]{1,0:T(8,128)(2,1)} %param.11) | copy-start | bytes 196612
  175.7 24.6 %copy-start.3 = (s32[8,16]{1,0:T(8,128)S(1)}, s32[8,16]{1,0:T(8,128)}, u32[]{:S(2)}) copy-start(s32[8,16]{1,0:T(8,128)} %param.12) | copy-start | bytes 1540
  175.7 116.7 %all-to-all-start.1 = ((bf16[64,2,32,256]{3,2,1,0:T(8,128)(2,1)}), bf16[64,2,32,256]{3,2,1,0:T(8,128)(2,1)}, u32[]{:S(2)}, u32[]{:S(2)}) async-start(bf16[64,2,32,256]{3,2,1,0:T(8,128)(2,1)} %broadcast_select_fusion), calls=%async_computation.1 | async-start | bytes 4194304 | tf_op jit(solution)/shard_map/all_to_all | solution.py:84
  185.8 137.8 %all-gather.5.cloned.1.call-start = ((), (), s32[]{:S(2)}) async-start(), calls=%async_computation.4 | async-start | bytes 4456448 | tf_op jit(solution)/shard_map/all_gather | solution.py:43
  302.2 2.6 copy-start.1
  308.1 15.5 %all-to-all-start.2 = ((bf16[2,256,512]{1,2,0:T(8,128)(2,1)}), bf16[2,256,512]{1,2,0:T(8,128)(2,1)S(1)}, u32[]{:S(2)}, u32[]{:S(2)}) async-start(bf16[2,256,512]{1,2,0:T(8,128)(2,1)} %broadcast_in_dim.118), calls=%async_computation.2 | async-start | bytes 1048576 | tf_op jit(solution)/shard_map/all_to_all | solution.py:25
Sparse Core Ops, SparseCore 0:
  11.1 155.1 all-gather.2
Sparse Core Ops, SparseCore 1:
  200.0 123.6 all-gather.4
where the time goes:
time: 336 us; the launch traced here: 335 us
  waiting for transfers between devices  219 us (65%)
  blocking collectives  47.2 us (14%)
  matrix products  17.1 us (5%)
  between operations  15.8 us (5%)
  other arithmetic  14.6 us (4%)
  starting transfers between devices  13.6 us (4%)
  local copies, waits for them, and re-layouts  7.73 us (2%)
    all_gather x1, waiting for transfers between devices, side_by_side(): filled, at, outs = (lax.all_gather(both, axis, axis=dim, tiled=True), 0, [])  121 us
    all_to_all x1, waiting for transfers between devices, body(): lax.all_to_all(outgoing, KV, split_axis=0, concat_axis=0, tiled=True)  86.4 us
    all_to_all x1, blocking collectives, body(): lax.all_to_all(wanted, KV, split_axis=0, concat_axis=0, tiled=True)  33.3 us
    all_gather x1, blocking collectives, gathered_by_axis(): shard = lax.all_gather(shard, axis, axis=dim, tiled=True)  14 us
    all_gather x1, waiting for transfers between devices, gathered_by_axis(): shard = lax.all_gather(shard, axis, axis=dim, tiled=True)  12 us
    all_to_all x1, starting transfers between devices, body(): lax.all_to_all(outgoing, KV, split_axis=0, concat_axis=0, tiled=True)  10.1 us
    dot_general x3, matrix products, add_rows(): return jnp.dot(tokens, piece, preferred_element_type=jnp.float32)  7.59 us
  transfers between devices with their start and end apart: 4, of which 3 were waited for; matrix products, arithmetic and copies ran while one was open for 7% of the time, Pallas kernels for 0%

commit v1 on v0

--- a/solution.py
+++ b/solution.py
@@ -9,15 +9,6 @@
 CAP = 2
 KV = ("kv_0", "kv_1")
 DP_KV = ("dp", "kv_0", "kv_1")
-
-
-def side_by_side(arrays, axis, dim, along):
-    both = jnp.concatenate(arrays, axis=along)
-    filled, at, outs = (lax.all_gather(both, axis, axis=dim, tiled=True), 0, [])
-    for a in arrays:
-        outs.append(lax.slice_in_dim(filled, at, at + a.shape[along], axis=along))
-        at += a.shape[along]
-    return tuple(outs)
 
 
 def copy_for_each(shard, axis):
@@ -38,10 +29,15 @@
     return laid_out(blocks, dim)
 
 
-def gathered_by_axis(shard, axes, dim):
-    for axis in reversed(axes):
-        shard = lax.all_gather(shard, axis, axis=dim, tiled=True)
-    return shard
+def spread_rows(shard):
+    planes = lax.axis_size("dp")
+    rows = shard.shape[0] // planes
+    mine = lax.dynamic_slice_in_dim(shard, lax.axis_index("dp") * rows, rows, axis=0)
+    column = copy_for_each(mine, "kv_0")
+    every = copy_for_each(column, ("dp", "kv_1"))
+    tall, wide = column.shape[0], lax.axis_size("kv_1")
+    every = every.reshape(planes, wide, tall, rows, -1)
+    return jnp.transpose(every, (2, 1, 0, 3, 4)).reshape(tall * wide * planes * rows, -1)
 
 
 def body(tokens, query_weight, key_weight, value_weight, out_weight, chosen, live_length):
@@ -53,12 +49,10 @@
     def add_rows(piece):
         return jnp.dot(tokens, piece, preferred_element_type=jnp.float32)
 
-    pieces = side_by_side((query_weight, key_weight, value_weight), KV, 0, 1)
-    queries = add_rows(pieces[0])
-    keys = add_rows(pieces[1])
-    values = add_rows(pieces[2])
-    queries = queries.astype(jnp.bfloat16)
-    paired = jnp.concatenate([keys.astype(jnp.bfloat16), values.astype(jnp.bfloat16)], axis=1)
+    paired = add_rows(
+        spread_rows(jnp.concatenate([key_weight, value_weight], axis=1))
+    ).astype(jnp.bfloat16)
+    queries = add_rows(lax.all_gather(query_weight, KV, axis=0, tiled=True)).astype(jnp.bfloat16)
     width = paired.shape[1]
     local_blocks = paired.reshape(per_dev, BLOCK, width)
     valid = chosen >= 0
@@ -120,7 +114,7 @@
     attended = result.astype(jnp.bfloat16).reshape(rows, -1)
     every_head = gathered_copies(attended, "tp", 1)
     mixed = jnp.dot(
-        every_head, gathered_by_axis(out_weight, KV, 0), preferred_element_type=jnp.float32
+        every_head, lax.all_gather(out_weight, KV, axis=0, tiled=True), preferred_element_type=jnp.float32
     )
     return mixed.astype(jnp.bfloat16)
 

time: 336 us -> 376 us (1.12)
  waiting for transfers between devices: 219 us -> 270 us
  blocking collectives: 47.2 us -> 16.8 us
  starting transfers between devices: 13.6 us -> 36.2 us
  local copies, waits for them, and re-layouts: 7.73 us -> 11.6 us
    all_gather x2, waiting for transfers between devices: 133 us -> 224 us  [the longest x1 119 us: body(): lax.all_gather(out_weight, KV, axis=0, tiled=True)]
    all_to_all x1, waiting for transfers between devices: 86.4 us -> 6.65 us  [body(): lax.all_to_all(outgoing, KV, split_axis=0, concat_axis=0, tiled=True)]
    all_to_all x1 -> x2, waiting for transfers between devices: 0.01 us -> 24 us  [copy_for_each(): lax.all_to_all(jnp.broadcast_to(shard[None], (count, *shard.shape)), axis...]
    all_to_all x0 -> x1, starting transfers between devices: none -> 18.7 us  [body(): lax.all_to_all(wanted, KV, split_axis=0, concat_axis=0, tiled=True)]
    all_to_all x1, blocking collectives: 33.3 us -> 16.8 us  [copy_for_each(): lax.all_to_all(jnp.broadcast_to(shard[None], (count, *shard.shape)), axis...]
    all_gather x1 -> x0, blocking collectives: 14 us -> none  [gathered_by_axis(): shard = lax.all_gather(shard, axis, axis=dim, tiled=True)]
    all_to_all x0 -> x1, waiting for transfers between devices: none -> 13.8 us  [body(): lax.all_to_all(wanted, KV, split_axis=0, concat_axis=0, tiled=True)]
    all_to_all x1 -> x2, starting transfers between devices: 3.49 us -> 8.91 us  [copy_for_each(): lax.all_to_all(jnp.broadcast_to(shard[None], (count, *shard.shape)), axis...]
  transfers between devices with their start and end apart: 4 -> 6, of which waited for: 3 -> 5; matrix products, arithmetic and copies ran while one was open for 7% -> 9% of each run, Pallas kernels for 0% -> 0%
where the time goes in v1:
time: 376 us
  waiting for transfers between devices  270 us (72%)
  starting transfers between devices  36.2 us (10%)
  blocking collectives  16.8 us (4%)
  between operations  14.3 us (4%)
  matrix products  13.7 us (4%)
  other arithmetic  13.5 us (4%)
  local copies, waits for them, and re-layouts  11.6 us (3%)
    all_gather x1, waiting for transfers between devices, body(): lax.all_gather(out_weight, KV, axis=0, tiled=True)  119 us
    all_gather x1, waiting for transfers between devices, body(): lax.all_gather(query_weight, KV, axis=0, tiled=True)  105 us
    all_to_all x2, waiting for transfers between devices, copy_for_each(): lax.all_to_all(jnp.broadcast_to(shard[None], (count, *shard.shape)), axis...  24 us
    all_to_all x1, starting transfers between devices, body(): lax.all_to_all(wanted, KV, split_axis=0, concat_axis=0, tiled=True)  18.7 us
    all_to_all x1, blocking collectives, copy_for_each(): lax.all_to_all(jnp.broadcast_to(shard[None], (count, *shard.shape)), axis...  16.8 us
    all_to_all x1, waiting for transfers between devices, body(): lax.all_to_all(wanted, KV, split_axis=0, concat_axis=0, tiled=True)  13.8 us
    all_to_all x2, starting transfers between devices, copy_for_each(): lax.all_to_all(jnp.broadcast_to(shard[None], (count, *shard.shape)), axis...  8.91 us
    all_to_all x1, starting transfers between devices, body(): lax.all_to_all(outgoing, KV, split_axis=0, concat_axis=0, tiled=True)  8.55 us
  transfers between devices with their start and end apart: 6, of which 5 were waited for; matrix products, arithmetic and copies ran while one was open for 9% of the time, Pallas kernels for 0%

profile of v1, /device:TPU:2, one launch (start us, length us, event | category | flops | bytes accessed | tf_op | source)
XLA Modules:
  0.0 375.7 jit_solution(15250901952565097661)
XLA Ops:
  6.5 0.7 all-gather.3.cloned.1.call-update
  7.3 0.7 broadcast_compare_fusion.1
  8.0 0.7 add_select_fusion.1
  9.1 0.2 select_reduce_fusion.2
  9.6 0.7 copy.37
  10.3 18.7 %all-to-all-start = ((s32[64,1,2]{2,1,0:T(1,128)}), s32[64,1,2]{2,1,0:T(1,128)S(1)}, u32[]{:S(2)}, u32[]{:S(2)}) async-start(s32[64,1,2]{2,1,0:T(1,128)} %copy.37), calls=%async_computation | async-start | bytes 65536 | tf_op jit(solution)/shard_map/all_to_all | solution.py:75
  29.1 0.7 fusion.22
  29.8 13.8 %all-to-all-done = s32[64,1,2]{2,1,0:T(1,128)S(1)} async-done(((s32[64,1,2]{2,1,0:T(1,128)}), s32[64,1,2]{2,1,0:T(1,128)S(1)}, u32[]{:S(2)}, u32[]{:S(2)}) %all-to-all-start) | async-done | bytes 544 | tf_op jit(solution)/shard_map/all_to_all | solution.py:75
  43.6 16.8 %all_to_all.29 = bf16[16,16,256]{2,1,0:T(8,128)(2,1)S(1)} all-to-all(bf16[16,16,256]{2,1,0:T(8,128)(2,1)S(1)} %broadcast_in_dim.122), channel_id=1, replica_groups=mesh['dp'=4,'kv_0'=16,'kv_1'=4,'tp'=2] {'kv_0'}, dimensions={0} | all-to-all | bytes 262144 | tf_op jit(solution)/shard_map/all_to_all | solution.py:16
  60.4 1.5 broadcast_in_dim.123
  61.9 5.4 %all-to-all-start.2 = ((bf16[16,16,16,256]{3,2,1,0:T(8,128)(2,1)}), bf16[16,16,16,256]{3,2,1,0:T(8,128)(2,1)}, u32[]{:S(2)}, u32[]{:S(2)}) async-start(bf16[16,16,16,256]{3,2,1,0:T(8,128)(2,1)} %broadcast_in_dim.123), calls=%async_computation.2 | async-start | bytes 4194304 | tf_op jit(solution)/shard_map/all_to_all | solution.py:16
  67.9 24.0 %all-to-all-done.2 = bf16[16,16,16,256]{3,2,1,0:T(8,128)(2,1)} async-done(((bf16[16,16,16,256]{3,2,1,0:T(8,128)(2,1)}), bf16[16,16,16,256]{3,2,1,0:T(8,128)(2,1)}, u32[]{:S(2)}, u32[]{:S(2)}) %all-to-all-start.2) | async-done | bytes 2097184 | tf_op jit(solution)/shard_map/all_to_all | solution.py:16
  91.9 1.9 copy.40
  93.8 0.7 convolution_convert_fusion.2
  94.5 2.0 gather_fusion
  96.5 3.1 broadcast_select_fusion
  99.6 8.6 %all-to-all-start.3 = ((bf16[64,2,32,256]{3,2,1,0:T(8,128)(2,1)}), bf16[64,2,32,256]{3,2,1,0:T(8,128)(2,1)}, u32[]{:S(2)}, u32[]{:S(2)}) async-start(bf16[64,2,32,256]{3,2,1,0:T(8,128)(2,1)} %broadcast_select_fusion), calls=%async_computation.3 | async-start | bytes 4194304 | tf_op jit(solution)/shard_map/all_to_all | solution.py:78
  108.2 0.7 all-gather.5.cloned.1.call-update
  109.0 0.3 select_reduce_fusion
  110.4 1.0 compare_and_fusion
  111.4 105.0 %all-gather.3.cloned.1.call-done = bf16[4096,512]{1,0:T(8,128)(2,1)} async-done(((bf16[64,512]{1,0:T(8,128)(2,1)}), bf16[4096,512]{1,0:T(8,128)(2,1)}) %all-gather.3.cloned.1.call-update) | async-done | bytes 4194320 | tf_op jit(solution)/shard_map/all_gather | solution.py:55
  216.4 3.4 convolution_convert_fusion.1
  219.9 6.6 %all-to-all-done.3 = bf16[64,2,32,256]{3,2,1,0:T(8,128)(2,1)} async-done(((bf16[64,2,32,256]{3,2,1,0:T(8,128)(2,1)}), bf16[64,2,32,256]{3,2,1,0:T(8,128)(2,1)}, u32[]{:S(2)}, u32[]{:S(2)}) %all-to-all-start.3) | async-done | bytes 2097184 | tf_op jit(solution)/shard_map/all_to_all | solution.py:78
  226.6 3.2 pad_maximum_fusion
  229.7 3.7 gather_fusion.1
  233.4 2.9 fusion.2
  236.4 2.5 fusion
  238.9 2.2 fusion.16
  241.4 0.8 broadcast_in_dim.132
  242.3 3.5 all-to-all-start.4
  245.8 118.7 %all-gather.5.cloned.1.call-done = bf16[1024,2048]{1,0:T(8,128)(2,1)} async-done(((bf16[16,2048]{1,0:T(8,128)(2,1)}), bf16[1024,2048]{1,0:T(8,128)(2,1)}) %all-gather.5.cloned.1.call-update) | async-done | bytes 4194320 | tf_op jit(solution)/shard_map/all_gather | solution.py:117
  364.4 4.4 %convolution_convert_fusion = bf16[256,2048]{1,0:T(8,128)(2,1)} fusion(bf16[256,1024]{0,1:T(8,128)(2,1)S(1)} %bitcast.93, bf16[1024,2048]{1,0:T(8,128)(2,1)} %all-gather.5.cloned.1.call-done), kind=kOutput, calls=%fused_computation.9 | convolution fusion | flops 1074266112 | bytes 5767168 | tf_op jit(solution)/shard_map/dot_general | solution.py:116
  (38 shorter events, 2.1 us)
Async XLA Ops:
  6.5 87.2 %copy-start = (bf16[256,4096]{1,0:T(8,128)(2,1)S(1)}, bf16[256,4096]{1,0:T(8,128)(2,1)}, u32[]{:S(2)}) copy-start(bf16[256,4096]{1,0:T(8,128)(2,1)} %param.7) | copy-start | bytes 6291460
  6.5 209.9 %all-gather.3.cloned.1.call-start = ((), (), s32[]{:S(2)}) async-start(), calls=%async_computation.5 | async-start | bytes 4259840 | tf_op jit(solution)/shard_map/all_gather | solution.py:55
  10.3 33.3 %all-to-all-start = ((s32[64,1,2]{2,1,0:T(1,128)}), s32[64,1,2]{2,1,0:T(1,128)S(1)}, u32[]{:S(2)}, u32[]{:S(2)}) async-start(s32[64,1,2]{2,1,0:T(1,128)} %copy.37), calls=%async_computation | async-start | bytes 65536 | tf_op jit(solution)/shard_map/all_to_all | solution.py:75
  61.9 29.9 %all-to-all-start.2 = ((bf16[16,16,16,256]{3,2,1,0:T(8,128)(2,1)}), bf16[16,16,16,256]{3,2,1,0:T(8,128)(2,1)}, u32[]{:S(2)}, u32[]{:S(2)}) async-start(bf16[16,16,16,256]{3,2,1,0:T(8,128)(2,1)} %broadcast_in_dim.123), calls=%async_computation.2 | async-start | bytes 4194304 | tf_op jit(solution)/shard_map/all_to_all | solution.py:16
  99.6 9.7 %copy-start.2 = (s32[8,16]{1,0:T(8,128)S(1)}, s32[8,16]{1,0:T(8,128)}, u32[]{:S(2)}) copy-start(s32[8,16]{1,0:T(8,128)} %param.12) | copy-start | bytes 1540
  99.6 126.9 %all-to-all-start.3 = ((bf16[64,2,32,256]{3,2,1,0:T(8,128)(2,1)}), bf16[64,2,32,256]{3,2,1,0:T(8,128)(2,1)}, u32[]{:S(2)}, u32[]{:S(2)}) async-start(bf16[64,2,32,256]{3,2,1,0:T(8,128)(2,1)} %broadcast_select_fusion), calls=%async_computation.3 | async-start | bytes 4194304 | tf_op jit(solution)/shard_map/all_to_all | solution.py:78
  108.2 256.2 %all-gather.5.cloned.1.call-start = ((), (), s32[]{:S(2)}) async-start(), calls=%async_computation.6 | async-start | bytes 4259840 | tf_op jit(solution)/shard_map/all_gather | solution.py:117
  236.3 2.6 copy-start.1
  242.3 122.2 %all-to-all-start.4 = ((bf16[2,256,512]{1,2,0:T(8,128)(2,1)}), bf16[2,256,512]{1,2,0:T(8,128)(2,1)S(1)}, u32[]{:S(2)}, u32[]{:S(2)}) async-start(bf16[2,256,512]{1,2,0:T(8,128)(2,1)} %broadcast_in_dim.132), calls=%async_computation.4 | async-start | bytes 1048576 | tf_op jit(solution)/shard_map/all_to_all | solution.py:16
Sparse Core Ops, SparseCore 0:
  10.3 206.0 all-gather.2
  219.4 145.0 all-gather.4
